TPU v7x, 32 devices: a whole 2x2x4 slice. The times are simulated.
32 devices in a mesh: ep: 4 (over y, x), tp: 8 (over z, core).
Axes of the slice: x: 2, y: 2, z: 4, core: 2. Of those that a mesh axis runs over, the one named last changes fastest.
Arguments:
- pool_input: bfloat16 [4096, 1024], P('ep', 'tp'), may hold values from -6 to 6
- pool_gain: float32 [1024], P('tp'), may hold values from 0.1 to 1.9
- mix_weight: bfloat16 [1024, 2048], P('tp'), may hold values from -0.1875 to 0.1875
- moe_input: bfloat16 [8192, 2048], P(('ep', 'tp')), may hold values from -6 to 6
- moe_gain: float32 [2048], replicated, may hold values from 0.1 to 1.9
- expert_ids: int32 [8192, 2], P(('ep', 'tp')), may hold values from 0 to 15, as said below
- route_weight: float32 [8192, 2], P(('ep', 'tp')), may hold values from 0.2 to 1
- gate_weight: bfloat16 [16, 2048, 1024], P('ep', None, 'tp'), may hold values from -0.125 to 0.125
- up_weight: bfloat16 [16, 2048, 1024], P('ep', None, 'tp'), may hold values from -0.125 to 0.125
- down_weight: bfloat16 [16, 2048, 1024], P('ep', None, 'tp'), may hold values from -0.1875 to 0.1875
Outputs:
- mixed_out: bfloat16 [4096, 2048], P(('ep', 'tp'))
- moe_out: bfloat16 [8192, 2048], P(('ep', 'tp'))
Inputs may be any that keep to these rules, and one draw needn't show every extreme that they name: `expert_ids`: each row names 2 different experts of one group of 4 consecutive experts. In each aligned block of 256 rows (the rows of one device) no expert is named by more than 48 rows, and some expert is named by exactly 48 rows.
All inputs are finite; a program needn't handle non-finite values.
Results may differ from a plain program's by a relative error of at most 0.012.
Values may be sent and summed in bfloat16 or wider, within the bound.
A program may use at most 128 MiB of HBM per device.

v0:
```python
import jax
import jax.numpy as jnp
from jax import lax
from jax.sharding import PartitionSpec as P

GROUP_CH = 256
EXPERTS = 16
TOP = 2
CAP = 48


eps_norm = 1e-06


def from_behind(shard, axis, by):
    peers = lax.axis_size(axis)
    pairs = [(i, i + by) for i in range(peers) if 0 <= i + by < peers]
    return lax.ppermute(shard, axis, pairs)


def window_sums(extended, row_count):
    level_sum = extended
    stride = 1
    outputs = []
    for doubling in range(4):
        level_sum = level_sum[stride:] + level_sum[:-stride]
        stride = stride * 2
        outputs.append(level_sum[level_sum.shape[0] - row_count :])
    return outputs


def pool_mixer(pool_input, pool_gain):
    row_count, channels = pool_input.shape
    carried = from_behind(pool_input[row_count - 15 :], "ep", 1)
    extended = jnp.concatenate([carried, pool_input], axis=0).astype(jnp.float32)
    window_list = window_sums(extended, row_count)
    channel_ids = lax.axis_index("tp") * channels + lax.iota(jnp.int32, channels)
    group_ids = channel_ids // GROUP_CH
    position = lax.axis_index("ep") * row_count + lax.iota(jnp.int32, row_count)
    summed = jnp.zeros((row_count, channels), jnp.float32)
    widths = jnp.zeros((channels,), jnp.int32)
    for index_group in range(4):
        inside = group_ids == index_group
        summed = jnp.where(inside[None, :], window_list[index_group], summed)
        widths = jnp.where(inside, 2 ** (index_group + 1), widths)
    counted = jnp.minimum(position[:, None] + 1, widths[None, :]).astype(jnp.float32)
    values = extended[15:]
    return ((summed / counted - values) * pool_gain).astype(jnp.bfloat16)


def route_slots(expert_ids):
    flat_ids = expert_ids.reshape(-1)
    marked = (flat_ids[:, None] == lax.iota(jnp.int32, EXPERTS)[None, :]).astype(jnp.int32)
    before_count = jnp.cumsum(marked, axis=0) - marked
    ranked = jnp.sum(before_count * marked, axis=1)
    return (flat_ids * CAP + ranked).reshape(expert_ids.shape)


def body(
    pool_input,
    pool_gain,
    mix_weight,
    moe_input,
    moe_gain,
    expert_ids,
    route_weight,
    gate_weight,
    up_weight,
    down_weight,
):
    pooled = pool_mixer(pool_input, pool_gain)
    regrouped = lax.all_to_all(pooled, "tp", split_axis=0, concat_axis=1, tiled=True)
    mixed_sum = jnp.dot(
        regrouped,
        lax.all_gather(mix_weight, "tp", axis=0, tiled=True),
        preferred_element_type=jnp.float32,
    )
    mixed_out = mixed_sum.astype(jnp.bfloat16)
    inputs = moe_input.astype(jnp.float32)
    scale_rows = lax.rsqrt(jnp.mean(inputs * inputs, axis=-1, keepdims=True) + eps_norm)
    normed = (inputs * scale_rows * moe_gain).astype(jnp.bfloat16)
    slots = route_slots(expert_ids)
    slot_index = lax.iota(jnp.int32, EXPERTS * CAP)
    placing = (
        (slot_index[:, None] == slots[None, :, 0]) | (slot_index[:, None] == slots[None, :, 1])
    ).astype(jnp.bfloat16)
    outgoing = jnp.dot(placing, normed, preferred_element_type=jnp.float32).astype(jnp.bfloat16)
    outgoing = outgoing.reshape(EXPERTS, CAP, normed.shape[1])
    arrived = lax.all_to_all(outgoing, "ep", split_axis=0, concat_axis=1, tiled=True)
    gate_piece = lax.all_gather(gate_weight, "tp", axis=2, tiled=True)
    up_piece = lax.all_gather(up_weight, "tp", axis=2, tiled=True)
    down_piece = lax.all_gather(down_weight, "tp", axis=2, tiled=True)
    gate_part = jnp.einsum("erd,edf->erf", arrived, gate_piece, preferred_element_type=jnp.float32)
    upward = jnp.einsum("erd,edf->erf", arrived, up_piece, preferred_element_type=jnp.float32)
    hidden = (jax.nn.silu(gate_part) * upward).astype(jnp.bfloat16)
    expert_sum = jnp.einsum("erf,edf->erd", hidden, down_piece, preferred_element_type=jnp.float32)
    expert_rows = expert_sum.astype(jnp.bfloat16)
    returned = lax.all_to_all(expert_rows, "ep", split_axis=1, concat_axis=0, tiled=True)
    returned_rows = returned.reshape(EXPERTS * CAP, returned.shape[2])
    combined = jnp.zeros((normed.shape[0], normed.shape[1]), jnp.float32)
    for route_index in range(TOP):
        picking = (slots[:, route_index][:, None] == slot_index[None, :]).astype(jnp.bfloat16)
        chosen_rows = jnp.dot(picking, returned_rows, preferred_element_type=jnp.float32)
        combined = combined + route_weight[:, route_index : route_index + 1] * chosen_rows
    moe_out = combined.astype(jnp.bfloat16)
    return (mixed_out, moe_out)


def solution(mesh):
    return jax.shard_map(
        body,
        mesh=mesh,
        in_specs=(
            P("ep", "tp"),
            P("tp"),
            P("tp", None),
            P(("ep", "tp"), None),
            P(),
            P(("ep", "tp"), None),
            P(("ep", "tp"), None),
            P("ep", None, "tp"),
            P("ep", None, "tp"),
            P("ep", None, "tp"),
        ),
        out_specs=(P(("ep", "tp"), None), P(("ep", "tp"), None)),
        check_vma=False,
    )
```

profile of v0, /device:TPU:0, one launch (start us, length us, event | category | flops | bytes accessed | tf_op | source)
XLA Modules:
  0.0 554.3 jit_solution(15557223583954882724)
XLA Ops:
  9.9 1.2 reduce-window.6
  12.0 2.8 convolution_convert_fusion
  14.7 5.3 all-to-all-start.1
  20.1 3.9 collective-permute-start
  24.1 30.0 %collective-permute-done = bf16[15,128]{1,0:T(8,128)(2,1)S(1)} collective-permute-done((bf16[15,128]{1,0:T(8,128)(2,1)S(1)}, bf16[15,128]{1,0:T(8,128)(2,1)S(1)}, u32[]{:S(2)}, u32[]{:S(2)}) %collective-permute-start) | collective-permute-done | bytes 3872 | tf_op jit(solution)/shard_map/ppermute | solution.py:18
  54.4 1.1 fusion.12
  55.4 0.8 all-to-all-done.1
  56.2 5.2 all-to-all-start
  61.4 1.9 copy.51
  63.3 107.9 %all-gather.7.cloned.1.call-done = bf16[4,2048,1024]{2,1,0:T(8,128)(2,1)} async-done(((bf16[4,2048,128]{2,1,0:T(8,128)(2,1)}), bf16[4,2048,1024]{2,1,0:T(8,128)(2,1)}) %all-gather.7.cloned.1.call-update) | async-done | bytes 16777232 | tf_op jit(solution)/shard_map/all_gather | solution.py:90
  171.2 11.9 %fusion.28 = f32[4,192,1024]{2,1,0:T(8,128)} fusion(bf16[4,192,2048]{2,1,0:T(8,128)(2,1)} %bitcast.48, bf16[4,2048,1024]{2,1,0:T(8,128)(2,1)} %all-gather.7.cloned.1.call-done), kind=kOutput, calls=%fused_computation.62 | convolution fusion | flops 3221225472 | bytes 23068672 | tf_op jit(solution)/shard_map/erd,edf->erf/dot_general | solution.py:93
  183.2 142.6 %all-gather.11.cloned.1.call-done = bf16[4,2048,1024]{2,1,0:T(8,128)(2,1)} async-done(((bf16[4,2048,128]{2,1,0:T(8,128)(2,1)}), bf16[4,2048,1024]{2,1,0:T(8,128)(2,1)}) %all-gather.11.cloned.1.call-update) | async-done | bytes 16777232 | tf_op jit(solution)/shard_map/all_gather | solution.py:92
  325.8 151.6 %all-gather.9.cloned.1.call-done = bf16[4,2048,1024]{2,1,0:T(8,128)(2,1)} async-done(((bf16[4,2048,128]{2,1,0:T(8,128)(2,1)}), bf16[4,2048,1024]{2,1,0:T(8,128)(2,1)}) %all-gather.9.cloned.1.call-update) | async-done | bytes 16777232 | tf_op jit(solution)/shard_map/all_gather | solution.py:91
  477.4 17.7 %convolution_convert_fusion.1 = bf16[4,192,2048]{2,1,0:T(8,128)(2,1)} fusion(bf16[4,2048,1024]{2,1,0:T(8,128)(2,1)} %all-gather.11.cloned.1.call-done, f32[4,192,1024]{2,1,0:T(8,128)} %fusion.28, bf16[4,192,2048]{2,1,0:T(8,128)(2,1)S(1)} %bitcast.49, bf16[4,2048,1024]{2,1,0:T(8,128)(2,1)} %all-gather.9.cloned.1.call-done), kind=kOutput, calls=%fused_computation.1 | convolution fusion | flops 6448742400 | bytes 42991616 | tf_op jit(solution)/shard_map/erf,edf->erd/dot_general | solution.py:96
  495.1 6.0 %copy.52 = bf16[4,192,2048]{2,0,1:T(4,128)(2,1)} copy(bf16[4,192,2048]{2,1,0:T(8,128)(2,1)} %convolution_convert_fusion.1) | data formatting | bytes 6291456 | tf_op jit(solution)/shard_map/convert_element_type | solution.py:97
  501.1 0.7 copy-done.2
  501.8 3.9 all-to-all-start.2
  505.7 1.1 copy.46
  506.9 17.0 %all-gather.5.cloned.1.call-done = bf16[1024,2048]{1,0:T(8,128)(2,1)} async-done(((bf16[128,2048]{1,0:T(8,128)(2,1)}), bf16[1024,2048]{1,0:T(8,128)(2,1)}) %all-gather.5.cloned.1.call-update) | async-done | bytes 4194320 | tf_op jit(solution)/shard_map/all_gather | solution.py:75
  523.9 3.7 convolution_convert_fusion.2
  527.6 14.8 %all-to-all-done.2 = bf16[4,192,2048]{2,0,1:T(4,128)(2,1)S(1)} async-done(((bf16[4,192,2048]{2,0,1:T(4,128)(2,1)}), bf16[4,192,2048]{2,0,1:T(4,128)(2,1)S(1)}, u32[]{:S(2)}, u32[]{:S(2)}) %all-to-all-start.2) | async-done | bytes 3145760 | tf_op jit(solution)/shard_map/all_to_all | solution.py:98
  542.5 1.7 copy.53
  544.6 1.0 convolution_multiply_fusion.1
  545.7 2.1 fusion.1
  (49 shorter events, 4.2 us)
Async XLA Ops:
  7.2 2.3 copy-start.5
  7.2 4.4 copy-start.1
  7.2 164.1 %all-gather.7.cloned.1.call-start = ((), (), s32[]{:S(2)}) async-start(), calls=%async_computation.4 | async-start | bytes 18874368 | tf_op jit(solution)/shard_map/all_gather | solution.py:90
  7.9 4.0 copy-start.4
  7.9 317.8 %all-gather.11.cloned.1.call-start = ((), (), s32[]{:S(2)}) async-start(), calls=%async_computation.6 | async-start | bytes 18874368 | tf_op jit(solution)/shard_map/all_gather | solution.py:92
  8.7 468.7 %all-gather.9.cloned.1.call-start = ((), (), s32[]{:S(2)}) async-start(), calls=%async_computation.5 | async-start | bytes 18874368 | tf_op jit(solution)/shard_map/all_gather | solution.py:91
  14.7 5.3 copy-start.3
  14.7 41.5 %all-to-all-start.1 = ((bf16[16,48,2048]{2,1,0:T(8,128)(2,1)}), bf16[16,48,2048]{2,1,0:T(8,128)(2,1)S(1)}, u32[]{:S(2)}, u32[]{:S(2)}) async-start(bf16[16,48,2048]{2,1,0:T(8,128)(2,1)} %bitcast.7), calls=%async_computation.1 | async-start | bytes 6291456 | tf_op jit(solution)/shard_map/all_to_all | solution.py:89
  20.0 34.3 %copy-start.7 = (f32[128]{0:T(128)S(1)}, f32[128]{0:T(128)}, u32[]{:S(2)}) copy-start(f32[128]{0:T(128)} %param.11) | copy-start | bytes 1540
  20.0 503.9 %all-gather.5.cloned.1.call-start = ((), (), s32[]{:S(2)}) async-start(), calls=%async_computation.3 | async-start | bytes 4718592 | tf_op jit(solution)/shard_map/all_gather | solution.py:75
  20.1 34.0 %collective-permute-start = (bf16[15,128]{1,0:T(8,128)(2,1)S(1)}, bf16[15,128]{1,0:T(8,128)(2,1)S(1)}, u32[]{:S(2)}, u32[]{:S(2)}) collective-permute-start(bf16[15,128]{1,0:T(8,128)(2,1)S(1)} %slice.57), channel_id=1, source_target_pairs={{0,8},{8,16},{16,24},{1,9},{9,17},{17,25},{2,10},{10,18},{18,26},{... | collective-permute-start | bytes 11528 | tf_op jit(solution)/shard_map/ppermute | solution.py:18
  56.2 444.9 %all-to-all-start = ((bf16[8,128,128]{2,1,0:T(8,128)(2,1)}), bf16[8,128,128]{2,1,0:T(8,128)(2,1)S(1)}, u32[]{:S(2)}, u32[]{:S(2)}) async-start(bf16[8,128,128]{2,1,0:T(8,128)(2,1)} %bitcast), calls=%async_computation | async-start | bytes 524288 | tf_op jit(solution)/shard_map/all_to_all | solution.py:72
  171.2 306.1 %copy-start = (bf16[4,4,48,2048]{3,2,0,1:T(8,128)(2,1)S(1)}, bf16[4,4,48,2048]{3,2,0,1:T(8,128)(2,1)}, u32[]{:S(2)}) copy-start(bf16[4,4,48,2048]{3,2,0,1:T(8,128)(2,1)} %copy.51) | copy-start | bytes 9437188
  501.1 4.6 copy-start.6
  501.1 0.7 copy-start.2
  501.8 40.6 %all-to-all-start.2 = ((bf16[4,192,2048]{2,0,1:T(4,128)(2,1)}), bf16[4,192,2048]{2,0,1:T(4,128)(2,1)S(1)}, u32[]{:S(2)}, u32[]{:S(2)}) async-start(bf16[4,192,2048]{2,0,1:T(4,128)(2,1)} %copy.52), calls=%async_computation.2 | async-start | bytes 6291456 | tf_op jit(solution)/shard_map/all_to_all | solution.py:98
Sparse Core Ops, SparseCore 0:
  9.6 161.6 all-gather.6
  172.8 152.8 all-gather.10
  327.4 149.9 all-gather.8
  478.8 45.0 all-gather.4
where the time goes:
time: 555 us; the launch traced here: 554 us
  waiting for transfers between devices  467 us (84%)
  matrix products  39.2 us (7%)
  starting transfers between devices  18.4 us (3%)
  between operations  14 us (3%)
  local copies, waits for them, and re-layouts  12.8 us (2%)
    all_gather x1, waiting for transfers between devices, body(): up_piece = lax.all_gather(up_weight, 'tp', axis=2, tiled=True)  152 us
    all_gather x1, waiting for transfers between devices, body(): down_piece = lax.all_gather(down_weight, 'tp', axis=2, tiled=True)  143 us
    all_gather x1, waiting for transfers between devices, body(): gate_piece = lax.all_gather(gate_weight, 'tp', axis=2, tiled=True)  108 us
    ppermute x1, waiting for transfers between devices, from_behind(): return lax.ppermute(shard, axis, pairs)  30 us
    dot_general x1, matrix products, body(): jnp.einsum('erf,edf->erd', hidden, down_piece, preferred_element_type=jnp...  17.7 us
    all_gather x1, waiting for transfers between devices, body(): lax.all_gather(mix_weight, 'tp', axis=0, tiled=True)  17 us
    all_to_all x1, waiting for transfers between devices, body(): lax.all_to_all(expert_rows, 'ep', split_axis=1, concat_axis=0, tiled=True)  14.8 us
    dot_general x1, matrix products, body(): jnp.einsum('erd,edf->erf', arrived, gate_piece, preferred_element_type=jn...  11.9 us
  transfers between devices with their start and end apart: 8, of which 7 were waited for; matrix products, arithmetic and copies ran while one was open for 9% of the time, Pallas kernels for 0%

commit v1 on v0

--- a/solution.py
+++ b/solution.py
@@ -5,6 +5,7 @@
 
 GROUP_CH = 256
 EXPERTS = 16
+GROUP_EXP = 4
 TOP = 2
 CAP = 48
 
@@ -48,12 +49,33 @@
     return ((summed / counted - values) * pool_gain).astype(jnp.bfloat16)
 
 
-def route_slots(expert_ids):
-    flat_ids = expert_ids.reshape(-1)
-    marked = (flat_ids[:, None] == lax.iota(jnp.int32, EXPERTS)[None, :]).astype(jnp.int32)
-    before_count = jnp.cumsum(marked, axis=0) - marked
-    ranked = jnp.sum(before_count * marked, axis=1)
-    return (flat_ids * CAP + ranked).reshape(expert_ids.shape)
+def dispatch_plan(expert_ids, route_weight, ep_size):
+    local_experts = EXPERTS // ep_size
+    share = TOP if local_experts % GROUP_EXP == 0 else 1
+    capacity = local_experts * CAP // share
+    owners = expert_ids // local_experts
+    ep_index = lax.iota(jnp.int32, ep_size)
+    member = jnp.any(owners[:, :, None] == ep_index[None, None, :], axis=1)
+    counts = member.astype(jnp.int32)
+    rank = jnp.cumsum(counts, axis=0) - counts
+    slot = jnp.where(member, rank, -1).T
+    placing = slot[:, None, :] == lax.iota(jnp.int32, capacity)[None, :, None]
+    dense_weight = jnp.sum(
+        jnp.where(
+            expert_ids[:, :, None] == lax.iota(jnp.int32, EXPERTS)[None, None, :],
+            route_weight[:, :, None],
+            0.0,
+        ),
+        axis=1,
+    )
+    dense_weight = dense_weight.reshape(-1, ep_size, local_experts)
+    slot_weight = jnp.einsum(
+        "ecn,nej->ecj",
+        placing.astype(jnp.float32),
+        dense_weight,
+        precision=lax.Precision.HIGHEST,
+    )
+    return placing.astype(jnp.bfloat16).reshape(ep_size * capacity, -1), slot_weight, capacity
 
 
 def body(
@@ -79,29 +101,25 @@
     inputs = moe_input.astype(jnp.float32)
     scale_rows = lax.rsqrt(jnp.mean(inputs * inputs, axis=-1, keepdims=True) + eps_norm)
     normed = (inputs * scale_rows * moe_gain).astype(jnp.bfloat16)
-    slots = route_slots(expert_ids)
-    slot_index = lax.iota(jnp.int32, EXPERTS * CAP)
-    placing = (
-        (slot_index[:, None] == slots[None, :, 0]) | (slot_index[:, None] == slots[None, :, 1])
-    ).astype(jnp.bfloat16)
+    ep_size = lax.axis_size("ep")
+    placing, slot_weight, capacity = dispatch_plan(expert_ids, route_weight, ep_size)
     outgoing = jnp.dot(placing, normed, preferred_element_type=jnp.float32).astype(jnp.bfloat16)
-    outgoing = outgoing.reshape(EXPERTS, CAP, normed.shape[1])
-    arrived = lax.all_to_all(outgoing, "ep", split_axis=0, concat_axis=1, tiled=True)
-    gate_piece = lax.all_gather(gate_weight, "tp", axis=2, tiled=True)
-    up_piece = lax.all_gather(up_weight, "tp", axis=2, tiled=True)
-    down_piece = lax.all_gather(down_weight, "tp", axis=2, tiled=True)
-    gate_part = jnp.einsum("erd,edf->erf", arrived, gate_piece, preferred_element_type=jnp.float32)
-    upward = jnp.einsum("erd,edf->erf", arrived, up_piece, preferred_element_type=jnp.float32)
-    hidden = (jax.nn.silu(gate_part) * upward).astype(jnp.bfloat16)
-    expert_sum = jnp.einsum("erf,edf->erd", hidden, down_piece, preferred_element_type=jnp.float32)
-    expert_rows = expert_sum.astype(jnp.bfloat16)
-    returned = lax.all_to_all(expert_rows, "ep", split_axis=1, concat_axis=0, tiled=True)
-    returned_rows = returned.reshape(EXPERTS * CAP, returned.shape[2])
-    combined = jnp.zeros((normed.shape[0], normed.shape[1]), jnp.float32)
-    for route_index in range(TOP):
-        picking = (slots[:, route_index][:, None] == slot_index[None, :]).astype(jnp.bfloat16)
-        chosen_rows = jnp.dot(picking, returned_rows, preferred_element_type=jnp.float32)
-        combined = combined + route_weight[:, route_index : route_index + 1] * chosen_rows
+    arrived = lax.all_to_all(outgoing, "ep", split_axis=0, concat_axis=0, tiled=True)
+    weights = lax.all_to_all(slot_weight, "ep", split_axis=0, concat_axis=0, tiled=True)
+    weights = weights.reshape(ep_size * capacity, -1)
+    tokens = lax.all_gather(arrived, "tp", axis=0, tiled=True)
+    weights = lax.all_gather(weights, "tp", axis=0, tiled=True)
+    gate_part = jnp.einsum("nd,edf->enf", tokens, gate_weight, preferred_element_type=jnp.float32)
+    upward = jnp.einsum("nd,edf->enf", tokens, up_weight, preferred_element_type=jnp.float32)
+    hidden = (jax.nn.silu(gate_part) * upward * weights.T[:, :, None]).astype(jnp.bfloat16)
+    partial = jnp.einsum("enf,edf->nd", hidden, down_weight, preferred_element_type=jnp.float32)
+    reduced = lax.psum_scatter(
+        partial.astype(jnp.bfloat16), "tp", scatter_dimension=0, tiled=True
+    )
+    returned = lax.all_to_all(reduced, "ep", split_axis=0, concat_axis=0, tiled=True)
+    combined = lax.dot_general(
+        placing, returned, (((0,), (0,)), ((), ())), preferred_element_type=jnp.float32
+    )
     moe_out = combined.astype(jnp.bfloat16)
     return (mixed_out, moe_out)
 

time: 555 us -> 380 us (0.68)
  waiting for transfers between devices: 467 us -> 246 us
  blocking collectives: 0 us -> 65.9 us
  local copies, waits for them, and re-layouts: 12.8 us -> 0.88 us
  starting transfers between devices: 18.4 us -> 7.76 us
    all_gather x3 -> x1, waiting for transfers between devices: 402 us -> 92 us  [body(): tokens = lax.all_gather(arrived, 'tp', axis=0, tiled=True)]
    reduce_scatter x0 -> x1, waiting for transfers between devices: none -> 109 us  [body(): lax.psum_scatter(partial.astype(jnp.bfloat16), 'tp', scatter_dimension=0,...]
    all_to_all x0 -> x3, blocking collectives: none -> 48.6 us  [the longest x1 24.9 us: body(): lax.all_to_all(outgoing, 'ep', split_axis=0, concat_axis=0, tiled=True)]
    ppermute x1, waiting for transfers between devices: 30 us -> 1.24 us  [from_behind(): return lax.ppermute(shard, axis, pairs)]
    all_gather x1, waiting for transfers between devices: 17 us -> 42.9 us  [body(): lax.all_gather(mix_weight, 'tp', axis=0, tiled=True)]
    all_gather x0 -> x1, blocking collectives: none -> 17.4 us  [body(): weights = lax.all_gather(weights, 'tp', axis=0, tiled=True)]
    all_to_all x3 -> x1, waiting for transfers between devices: 15.6 us -> 0.01 us  [body(): lax.all_to_all(reduced, 'ep', split_axis=0, concat_axis=0, tiled=True)]
    all_to_all x3 -> x1, starting transfers between devices: 14.4 us -> 4.34 us  [body(): lax.all_to_all(reduced, 'ep', split_axis=0, concat_axis=0, tiled=True)]
  transfers between devices with their start and end apart: 8 -> 5, of which waited for: 7 -> 4; matrix products, arithmetic and copies ran while one was open for 9% -> 1% of each run, Pallas kernels for 0% -> 0%
where the time goes in v1:
time: 380 us; the launch traced here: 379 us
  waiting for transfers between devices  246 us (65%)
  blocking collectives  65.9 us (17%)
  matrix products  40.5 us (11%)
  between operations  13.9 us (4%)
  starting transfers between devices  7.76 us (2%)
  other arithmetic  4.48 us (1%)
    reduce_scatter x1, waiting for transfers between devices, body(): lax.psum_scatter(partial.astype(jnp.bfloat16), 'tp', scatter_dimension=0,...  109 us
    all_gather x1, waiting for transfers between devices, body(): tokens = lax.all_gather(arrived, 'tp', axis=0, tiled=True)  92 us
    all_gather x1, waiting for transfers between devices, body(): lax.all_gather(mix_weight, 'tp', axis=0, tiled=True)  42.9 us
    all_to_all x1, blocking collectives, body(): lax.all_to_all(outgoing, 'ep', split_axis=0, concat_axis=0, tiled=True)  24.9 us
    dot_general x1, matrix products, body(): jnp.einsum('enf,edf->nd', hidden, down_weight, preferred_element_type=jnp...  19.4 us
    all_gather x1, blocking collectives, body(): weights = lax.all_gather(weights, 'tp', axis=0, tiled=True)  17.4 us
    all_to_all x1, blocking collectives, body(): lax.all_to_all(pooled, 'tp', split_axis=0, concat_axis=1, tiled=True)  16.7 us
    dot_general x1, matrix products, body(): jnp.einsum('nd,edf->enf', tokens, gate_weight, preferred_element_type=jnp...  12 us
  transfers between devices with their start and end apart: 5, of which 4 were waited for; matrix products, arithmetic and copies ran while one was open for 1% of the time, Pallas kernels for 0%

profile of v1, /device:TPU:0, one launch (start us, length us, event | category | flops | bytes accessed | tf_op | source)
XLA Modules:
  0.0 379.1 jit_solution(9585453362862034271)
XLA Ops:
  7.2 0.8 and_select_fusion
  8.1 1.2 reduce-window.6
  9.8 1.5 fusion.16
  11.3 0.1 bitcast_compare_fusion
  11.5 1.9 convolution_convert_fusion
  13.4 24.9 %all_to_all.45 = bf16[4,96,2048]{2,1,0:T(8,128)(2,1)} all-to-all(bf16[4,96,2048]{2,1,0:T(8,128)(2,1)S(1)} %bitcast.72), channel_id=1, replica_groups=mesh['ep'=4,'tp'=8] {'ep'}, dimensions={0} | all-to-all | bytes 3145728 | tf_op jit(solution)/shard_map/all_to_all | solution.py:107
  38.4 0.3 fusion.28
  38.7 7.0 %all_to_all.46 = f32[4,96,4]{1,2,0:T(4,128)S(1)} all-to-all(f32[4,96,4]{1,2,0:T(4,128)S(1)} %fusion.28), channel_id=1, replica_groups=mesh['ep'=4,'tp'=8] {'ep'}, dimensions={0} | all-to-all | bytes 12288 | tf_op jit(solution)/shard_map/all_to_all | solution.py:108
  45.8 17.4 %all_gather.11 = f32[3072,4]{0,1:T(4,128)S(1)} all-gather(f32[384,4]{0,1:T(4,128)S(1)} %reshape.89), channel_id=1, replica_groups=mesh['ep'=4,'tp'=8] {'tp'}, dimensions={0}, use_global_device_ids=true | all-gather | bytes 55296 | tf_op jit(solution)/shard_map/all_gather | solution.py:111
  63.2 92.0 %all-gather.5.cloned.1.call-done = bf16[3072,2048]{1,0:T(8,128)(2,1)} async-done(((bf16[384,2048]{1,0:T(8,128)(2,1)}), bf16[3072,2048]{1,0:T(8,128)(2,1)}) %all-gather.5.cloned.1.call-update) | async-done | bytes 12582928 | tf_op jit(solution)/shard_map/all_gather | solution.py:110
  155.2 12.0 %fusion.2 = f32[3072,4,128]{2,0,1:T(8,128)} fusion(bf16[4,2048,128]{2,1,0:T(8,128)(2,1)} %param.17, bf16[3072,2048]{1,0:T(8,128)(2,1)} %all-gather.5.cloned.1.call-done), kind=kOutput, calls=%fused_computation.3 | convolution fusion | flops 6442450944 | bytes 20971520 | tf_op jit(solution)/shard_map/nd,edf->enf/dot_general | solution.py:112
  167.2 19.4 %bitcast_convert_fusion = bf16[3072,2048]{1,0:T(8,128)(2,1)} fusion(bf16[4,2048,128]{2,1,0:T(8,128)(2,1)S(1)} %copy-done, f32[3072,4,128]{2,0,1:T(8,128)} %fusion.2, bf16[4,2048,128]{2,1,0:T(8,128)(2,1)} %param.18, bf16[3072,2048]{1,0:T(8,128)(2,1)} %all-gather.5.cloned.1.call-done, f32[4,3072]{1,0:T(4,128)S(1)} %bitcast.77), kind=kOutput, calls=%fused_computation | convolution fusion | flops 12902203392 | bytes 35700736 | tf_op jit(solution)/shard_map/enf,edf->nd/dot_general | solution.py:115
  186.7 0.7 all-gather.3.cloned.1.call-update
  187.4 0.2 copy-done.1
  187.6 3.3 collective-permute-start
  190.9 1.2 collective-permute-done
  192.4 0.4 fusion.23
  192.8 16.7 %all_to_all.47 = bf16[8,128,128]{2,1,0:T(8,128)(2,1)S(1)} all-to-all(bf16[8,128,128]{2,1,0:T(8,128)(2,1)S(1)} %bitcast.74), channel_id=1, replica_groups=mesh['ep'=4,'tp'=8] {'tp'}, dimensions={0} | all-to-all | bytes 524288 | tf_op jit(solution)/shard_map/all_to_all | solution.py:94
  209.5 108.7 %reduce-scatter.2.cloned.1.call-done = bf16[384,2048]{1,0:T(8,128)(2,1)} async-done(((bf16[3072,2048]{1,0:T(8,128)(2,1)}), bf16[384,2048]{1,0:T(8,128)(2,1)}) %reduce-scatter.2.cloned.1.call-update) | async-done | bytes 1572880 | tf_op jit(solution)/shard_map/reduce_scatter | solution.py:116
  318.2 4.3 %all-to-all-start.3 = ((bf16[4,96,2048]{2,1,0:T(8,128)(2,1)}), bf16[4,96,2048]{2,1,0:T(8,128)(2,1)}, u32[]{:S(2)}, u32[]{:S(2)}) async-start(bf16[4,96,2048]{2,1,0:T(8,128)(2,1)} %bitcast.73), calls=%async_computation.4 | async-start | bytes 3145728 | tf_op jit(solution)/shard_map/all_to_all | solution.py:119
  322.6 0.2 copy.30
  322.7 42.9 %all-gather.3.cloned.1.call-done = bf16[1024,2048]{1,0:T(8,128)(2,1)} async-done(((bf16[128,2048]{1,0:T(8,128)(2,1)}), bf16[1024,2048]{1,0:T(8,128)(2,1)}) %all-gather.3.cloned.1.call-update) | async-done | bytes 4194320 | tf_op jit(solution)/shard_map/all_gather | solution.py:97
  365.7 3.7 convolution_convert_fusion.1
  369.4 3.1 fusion.15
  (41 shorter events, 1.1 us)
Async XLA Ops:
  7.2 160.0 %copy-start = (bf16[4,2048,128]{2,1,0:T(8,128)(2,1)S(1)}, bf16[4,2048,128]{2,1,0:T(8,128)(2,1)}, u32[]{:S(2)}) copy-start(bf16[4,2048,128]{2,1,0:T(8,128)(2,1)} %param.19) | copy-start | bytes 6291460
  7.2 148.0 %all-gather.5.cloned.1.call-start = ((), (), s32[]{:S(2)}) async-start(), calls=%async_computation.6 | async-start | bytes 14155776 | tf_op jit(solution)/shard_map/all_gather | solution.py:110
  11.5 26.9 %copy-start.2 = (s32[256,2]{0,1:T(2,128)S(1)}, s32[256,2]{0,1:T(2,128)}, u32[]{:S(2)}) copy-start(s32[256,2]{0,1:T(2,128)} %param.15) | copy-start | bytes 6148
  11.5 26.9 %copy-start.3 = (f32[256,2]{0,1:T(2,128)S(1)}, f32[256,2]{0,1:T(2,128)}, u32[]{:S(2)}) copy-start(f32[256,2]{0,1:T(2,128)} %param.16) | copy-start | bytes 6148
  38.3 279.9 %reduce-scatter.2.cloned.1.call-start = ((), (), s32[]{:S(2)}) async-start(), calls=%async_computation.7 | async-start | bytes 14155776 | tf_op jit(solution)/shard_map/reduce_scatter | solution.py:116
  186.6 0.9 copy-start.1
  186.6 5.8 %copy-start.4 = (f32[128]{0:T(128)S(1)}, f32[128]{0:T(128)}, u32[]{:S(2)}) copy-start(f32[128]{0:T(128)} %param.11) | copy-start | bytes 1540
  186.6 179.0 %all-gather.3.cloned.1.call-start = ((), (), s32[]{:S(2)}) async-start(), calls=%async_computation.5 | async-start | bytes 4718592 | tf_op jit(solution)/shard_map/all_gather | solution.py:97
  187.6 4.6 %collective-permute-start = (bf16[15,128]{1,0:T(8,128)(2,1)S(1)}, bf16[15,128]{1,0:T(8,128)(2,1)S(1)}, u32[]{:S(2)}, u32[]{:S(2)}) collective-permute-start(bf16[15,128]{1,0:T(8,128)(2,1)S(1)} %slice.43), channel_id=1, source_target_pairs={{0,8},{8,16},{16,24},{1,9},{9,17},{17,25},{2,10},{10,18},{18,26},{... | collective-permute-start | bytes 11528 | tf_op jit(solution)/shard_map/ppermute | solution.py:19
  318.2 51.2 %all-to-all-start.3 = ((bf16[4,96,2048]{2,1,0:T(8,128)(2,1)}), bf16[4,96,2048]{2,1,0:T(8,128)(2,1)}, u32[]{:S(2)}, u32[]{:S(2)}) async-start(bf16[4,96,2048]{2,1,0:T(8,128)(2,1)} %bitcast.73), calls=%async_computation.4 | async-start | bytes 3145728 | tf_op jit(solution)/shard_map/all_to_all | solution.py:119
Sparse Core Ops, SparseCore 0:
  38.4 116.7 all-gather.4
  186.7 131.4 reduce-scatter.1
  319.8 45.8 all-gather.2

commit v2 on v1

--- a/solution.py
+++ b/solution.py
@@ -8,6 +8,7 @@
 GROUP_EXP = 4
 TOP = 2
 CAP = 48
+CHUNKS = 2
 
 
 eps_norm = 1e-06
@@ -91,36 +92,64 @@
     down_weight,
 ):
     pooled = pool_mixer(pool_input, pool_gain)
-    regrouped = lax.all_to_all(pooled, "tp", split_axis=0, concat_axis=1, tiled=True)
-    mixed_sum = jnp.dot(
-        regrouped,
-        lax.all_gather(mix_weight, "tp", axis=0, tiled=True),
-        preferred_element_type=jnp.float32,
+    ep_size = lax.axis_size("ep")
+    out_columns = mix_weight.shape[1] // ep_size
+    mix_columns = lax.dynamic_slice_in_dim(
+        mix_weight, lax.axis_index("ep") * out_columns, out_columns, axis=1
     )
-    mixed_out = mixed_sum.astype(jnp.bfloat16)
+    mix_columns = lax.all_gather(mix_columns, "tp", axis=0, tiled=True)
     inputs = moe_input.astype(jnp.float32)
     scale_rows = lax.rsqrt(jnp.mean(inputs * inputs, axis=-1, keepdims=True) + eps_norm)
     normed = (inputs * scale_rows * moe_gain).astype(jnp.bfloat16)
-    ep_size = lax.axis_size("ep")
     placing, slot_weight, capacity = dispatch_plan(expert_ids, route_weight, ep_size)
-    outgoing = jnp.dot(placing, normed, preferred_element_type=jnp.float32).astype(jnp.bfloat16)
-    arrived = lax.all_to_all(outgoing, "ep", split_axis=0, concat_axis=0, tiled=True)
+    rows = capacity // CHUNKS
+    arrived_list = []
+    placing_list = []
+    for chunk in range(CHUNKS):
+        chunk_placing = placing.reshape(ep_size, capacity, -1)[:, chunk * rows : (chunk + 1) * rows]
+        chunk_placing = chunk_placing.reshape(ep_size * rows, -1)
+        outgoing = jnp.dot(chunk_placing, normed, preferred_element_type=jnp.float32)
+        outgoing = outgoing.astype(jnp.bfloat16)
+        placing_list.append(chunk_placing)
+        arrived_list.append(
+            lax.all_to_all(outgoing, "ep", split_axis=0, concat_axis=0, tiled=True)
+        )
+    arrived_list[0], mix_columns = lax.optimization_barrier((arrived_list[0], mix_columns))
     weights = lax.all_to_all(slot_weight, "ep", split_axis=0, concat_axis=0, tiled=True)
-    weights = weights.reshape(ep_size * capacity, -1)
-    tokens = lax.all_gather(arrived, "tp", axis=0, tiled=True)
     weights = lax.all_gather(weights, "tp", axis=0, tiled=True)
-    gate_part = jnp.einsum("nd,edf->enf", tokens, gate_weight, preferred_element_type=jnp.float32)
-    upward = jnp.einsum("nd,edf->enf", tokens, up_weight, preferred_element_type=jnp.float32)
-    hidden = (jax.nn.silu(gate_part) * upward * weights.T[:, :, None]).astype(jnp.bfloat16)
-    partial = jnp.einsum("enf,edf->nd", hidden, down_weight, preferred_element_type=jnp.float32)
-    reduced = lax.psum_scatter(
-        partial.astype(jnp.bfloat16), "tp", scatter_dimension=0, tiled=True
+    combined = jnp.zeros(normed.shape, jnp.float32)
+    for chunk in range(CHUNKS):
+        tokens = lax.all_gather(arrived_list[chunk], "tp", axis=0, tiled=True)
+        scales = weights[:, chunk * rows : (chunk + 1) * rows].reshape(tokens.shape[0], -1)
+        gate_part = jnp.einsum(
+            "nd,edf->enf", tokens, gate_weight, preferred_element_type=jnp.float32
+        )
+        upward = jnp.einsum("nd,edf->enf", tokens, up_weight, preferred_element_type=jnp.float32)
+        hidden = (jax.nn.silu(gate_part) * upward * scales.T[:, :, None]).astype(jnp.bfloat16)
+        partial = jnp.einsum("enf,edf->nd", hidden, down_weight, preferred_element_type=jnp.float32)
+        reduced = lax.psum_scatter(
+            partial.astype(jnp.bfloat16), "tp", scatter_dimension=0, tiled=True
+        )
+        returned = lax.all_to_all(reduced, "ep", split_axis=0, concat_axis=0, tiled=True)
+        combined = combined + lax.dot_general(
+            placing_list[chunk],
+            returned,
+            (((0,), (0,)), ((), ())),
+            preferred_element_type=jnp.float32,
+        )
+    moe_out = combined.astype(jnp.bfloat16)
+    regrouped = lax.all_to_all(pooled, "tp", split_axis=0, concat_axis=1, tiled=True)
+    half = regrouped.shape[1] // 2
+    mixed_sum = 0.0
+    for part in range(2):
+        section = slice(part * half, (part + 1) * half)
+        pooled_rows = lax.all_gather(regrouped[:, section], "ep", axis=0, tiled=True)
+        mixed_sum = mixed_sum + jnp.dot(
+            pooled_rows, mix_columns[section], preferred_element_type=jnp.float32
+        )
+    mixed_out = lax.all_to_all(
+        mixed_sum.astype(jnp.bfloat16), "ep", split_axis=0, concat_axis=1, tiled=True
     )
-    returned = lax.all_to_all(reduced, "ep", split_axis=0, concat_axis=0, tiled=True)
-    combined = lax.dot_general(
-        placing, returned, (((0,), (0,)), ((), ())), preferred_element_type=jnp.float32
-    )
-    moe_out = combined.astype(jnp.bfloat16)
     return (mixed_out, moe_out)
 
 

time: 380 us -> 336 us (0.88)
  waiting for transfers between devices: 246 us -> 140 us
  blocking collectives: 65.9 us -> 113 us
  matrix products: 40.5 us -> 50.6 us
  local copies, waits for them, and re-layouts: 0.88 us -> 5.31 us
    all_gather x2 -> x3, waiting for transfers between devices: 135 us -> 78 us  [the longest x2 78 us: body(): tokens = lax.all_gather(arrived_list[chunk], 'tp', axis=0, tiled=True)]
    reduce_scatter x1 -> x2, waiting for transfers between devices: 109 us -> 55.6 us  [body(): lax.psum_scatter(partial.astype(jnp.bfloat16), 'tp', scatter_dimension=0,...]
    all_to_all x0 -> x2, blocking collectives: none -> 23.1 us  [the longest x1 12.8 us: body(): lax.all_to_all(reduced, 'ep', split_axis=0, concat_axis=0, tiled=True)]
    all_gather x0 -> x2, blocking collectives: none -> 20.8 us  [body(): lax.all_gather(regrouped[:, section], 'ep', axis=0, tiled=True)]
    all_to_all x1, waiting for transfers between devices: 0.01 us -> 5.3 us  [body(): lax.all_to_all(reduced, 'ep', split_axis=0, concat_axis=0, tiled=True)]
    dot_general x1 -> x2, matrix products: 12 us -> 17 us  [body(): jnp.einsum('nd,edf->enf', tokens, gate_weight, preferred_element_type=jnp...]
    all_to_all x1 -> x2, blocking collectives: 24.9 us -> 29.7 us  [body(): lax.all_to_all(outgoing, 'ep', split_axis=0, concat_axis=0, tiled=True)]
    dot_general x1 -> x2, matrix products: 19.4 us -> 24.1 us  [body(): jnp.einsum('enf,edf->nd', hidden, down_weight, preferred_element_type=jnp...]
  transfers between devices with their start and end apart: 5 -> 7, of which waited for: 4 -> 5; matrix products, arithmetic and copies ran while one was open for 1% -> 16% of each run, Pallas kernels for 0% -> 0%
where the time goes in v2:
time: 336 us; the launch traced here: 335 us
  waiting for transfers between devices  140 us (42%)
  blocking collectives  113 us (34%)
  matrix products  50.6 us (15%)
  between operations  14 us (4%)
  starting transfers between devices  7.53 us (2%)
  local copies, waits for them, and re-layouts  5.31 us (2%)
  other arithmetic  4.27 us (1%)
    all_gather x2, waiting for transfers between devices, body(): tokens = lax.all_gather(arrived_list[chunk], 'tp', axis=0, tiled=True)  78 us
    reduce_scatter x2, waiting for transfers between devices, body(): lax.psum_scatter(partial.astype(jnp.bfloat16), 'tp', scatter_dimension=0,...  55.6 us
    all_to_all x2, blocking collectives, body(): lax.all_to_all(outgoing, 'ep', split_axis=0, concat_axis=0, tiled=True)  29.7 us
    dot_general x2, matrix products, body(): jnp.einsum('enf,edf->nd', hidden, down_weight, preferred_element_type=jnp...  24.1 us
    all_gather x2, blocking collectives, body(): lax.all_gather(regrouped[:, section], 'ep', axis=0, tiled=True)  20.8 us
    all_to_all x1, blocking collectives, body(): lax.all_to_all(pooled, 'tp', split_axis=0, concat_axis=1, tiled=True)  17.3 us
    dot_general x2, matrix products, body(): jnp.einsum('nd,edf->enf', tokens, gate_weight, preferred_element_type=jnp...  17 us
    all_gather x1, blocking collectives, body(): weights = lax.all_gather(weights, 'tp', axis=0, tiled=True)  14.8 us
  transfers between devices with their start and end apart: 7, of which 5 were waited for; matrix products, arithmetic and copies ran while one was open for 16% of the time, Pallas kernels for 0%

profile of v2, /device:TPU:0, one launch (start us, length us, event | category | flops | bytes accessed | tf_op | source)
XLA Modules:
  0.0 334.8 jit_solution(6030024763773392144)
XLA Ops:
  7.3 1.7 constant_dynamic-slice_fusion
  9.8 1.5 fusion.40
  13.0 1.7 convolution_convert_fusion
  14.8 16.4 %all_to_all.85 = bf16[4,48,2048]{2,1,0:T(8,128)(2,1)} all-to-all(bf16[4,48,2048]{2,1,0:T(8,128)(2,1)S(1)} %bitcast.128), channel_id=1, replica_groups=mesh['ep'=4,'tp'=8] {'ep'}, dimensions={0} | all-to-all | bytes 1572864 | tf_op jit(solution)/shard_map/all_to_all | solution.py:115
  31.8 13.2 %all_to_all.86 = bf16[4,48,2048]{2,1,0:T(8,128)(2,1)} all-to-all(bf16[4,48,2048]{2,1,0:T(8,128)(2,1)S(1)} %bitcast.127), channel_id=1, replica_groups=mesh['ep'=4,'tp'=8] {'ep'}, dimensions={0} | all-to-all | bytes 1572864 | tf_op jit(solution)/shard_map/all_to_all | solution.py:115
  45.4 7.0 %all_to_all.87 = f32[4,96,4]{1,2,0:T(4,128)S(1)} all-to-all(f32[4,96,4]{1,2,0:T(4,128)S(1)} %fusion.65), channel_id=1, replica_groups=mesh['ep'=4,'tp'=8] {'ep'}, dimensions={0} | all-to-all | bytes 12288 | tf_op jit(solution)/shard_map/all_to_all | solution.py:118
  52.5 14.8 %all_gather.22 = f32[32,96,4]{1,2,0:T(4,128)S(1)} all-gather(f32[4,96,4]{1,2,0:T(4,128)S(1)} %all_to_all.87), channel_id=1, replica_groups=mesh['ep'=4,'tp'=8] {'tp'}, dimensions={0}, use_global_device_ids=true | all-gather | bytes 55296 | tf_op jit(solution)/shard_map/all_gather | solution.py:119
  67.5 34.2 %all-gather.8.cloned.1.call-done = bf16[1536,2048]{1,0:T(8,128)(2,1)} async-done(((bf16[192,2048]{1,0:T(8,128)(2,1)}), bf16[1536,2048]{1,0:T(8,128)(2,1)}) %all-gather.8.cloned.1.call-update) | async-done | bytes 6291472 | tf_op jit(solution)/shard_map/all_gather | solution.py:122
  101.7 8.5 %fusion.20 = f32[4,1536,128]{2,1,0:T(8,128)} fusion(bf16[4,2048,128]{2,1,0:T(8,128)(2,1)} %param.17, bf16[1536,2048]{1,0:T(8,128)(2,1)} %all-gather.8.cloned.1.call-done), kind=kOutput, calls=%fused_computation.14 | convolution fusion | flops 3221225472 | bytes 11534336 | tf_op jit(solution)/shard_map/nd,edf->enf/dot_general | solution.py:124
  110.2 12.3 %bitcast_convert_fusion = bf16[1536,2048]{1,0:T(8,128)(2,1)} fusion(bf16[4,2048,128]{2,1,0:T(8,128)(2,1)S(1)} %copy-done, bf16[4,2048,128]{2,1,0:T(8,128)(2,1)} %param.18, bf16[1536,2048]{1,0:T(8,128)(2,1)} %all-gather.8.cloned.1.call-done, f32[4,1536,128]{2,1,0:T(8,128)} %fusion.20, f32[4,1536]{1,0:T(4,128)S(1)} %bitcast.132), kind=kOutput, calls=%fused_computation | convolution fusion | flops 6451101696 | bytes 19947520 | tf_op jit(solution)/shard_map/enf,edf->nd/dot_general | solution.py:129
  122.9 43.8 %all-gather.6.cloned.1.call-done = bf16[1536,2048]{1,0:T(8,128)(2,1)} async-done(((bf16[192,2048]{1,0:T(8,128)(2,1)}), bf16[1536,2048]{1,0:T(8,128)(2,1)}) %all-gather.6.cloned.1.call-update) | async-done | bytes 6291472 | tf_op jit(solution)/shard_map/all_gather | solution.py:122
  166.7 8.5 %fusion.8 = f32[4,1536,128]{2,1,0:T(8,128)} fusion(bf16[4,2048,128]{2,1,0:T(8,128)(2,1)} %param.17, bf16[1536,2048]{1,0:T(8,128)(2,1)} %all-gather.6.cloned.1.call-done), kind=kOutput, calls=%fused_computation.10 | convolution fusion | flops 3221225472 | bytes 11534336 | tf_op jit(solution)/shard_map/nd,edf->enf/dot_general | solution.py:124
  175.3 11.8 %bitcast_convert_fusion.1 = bf16[1536,2048]{1,0:T(8,128)(2,1)} fusion(bf16[4,2048,128]{2,1,0:T(8,128)(2,1)S(1)} %copy-done, bf16[4,2048,128]{2,1,0:T(8,128)(2,1)} %param.18, bf16[1536,2048]{1,0:T(8,128)(2,1)} %all-gather.6.cloned.1.call-done, f32[4,1536,128]{2,1,0:T(8,128)} %fusion.8, f32[4,1536]{1,0:T(4,128)S(1)} %bitcast.133), kind=kOutput, calls=%fused_computation.1 | convolution fusion | flops 6451101696 | bytes 19947520 | tf_op jit(solution)/shard_map/enf,edf->nd/dot_general | solution.py:129
  188.0 3.5 %collective-permute-start = (bf16[15,128]{1,0:T(8,128)(2,1)S(1)}, bf16[15,128]{1,0:T(8,128)(2,1)S(1)}, u32[]{:S(2)}, u32[]{:S(2)}) collective-permute-start(bf16[15,128]{1,0:T(8,128)(2,1)S(1)} %slice.67), channel_id=1, source_target_pairs={{0,8},{8,16},{16,24},{1,9},{9,17},{17,25},{2,10},{10,18},{18,26},{... | collective-permute-start | bytes 11528 | tf_op jit(solution)/shard_map/ppermute | solution.py:20
  193.5 17.3 %all_to_all.88 = bf16[8,128,128]{2,1,0:T(8,128)(2,1)} all-to-all(bf16[8,128,128]{2,1,0:T(8,128)(2,1)S(1)} %bitcast.122), channel_id=1, replica_groups=mesh['ep'=4,'tp'=8] {'tp'}, dimensions={0} | all-to-all | bytes 524288 | tf_op jit(solution)/shard_map/all_to_all | solution.py:141
  212.0 11.7 %all_gather.18 = bf16[512,512]{0,1:T(8,128)(2,1)S(1)} all-gather(bf16[128,512]{0,1:T(8,128)(2,1)S(1)} %get-tuple-element.7), channel_id=1, replica_groups=mesh['ep'=4,'tp'=8] {'ep'}, dimensions={0}, use_global_device_ids=true | all-gather | bytes 655360 | tf_op jit(solution)/shard_map/all_gather | solution.py:146
  223.7 9.1 %all_gather.20 = bf16[512,512]{0,1:T(8,128)(2,1)S(1)} all-gather(bf16[128,512]{0,1:T(8,128)(2,1)S(1)} %get-tuple-element.6), channel_id=1, replica_groups=mesh['ep'=4,'tp'=8] {'ep'}, dimensions={0}, use_global_device_ids=true | all-gather | bytes 655360 | tf_op jit(solution)/shard_map/all_gather | solution.py:146
  233.7 10.3 %all_to_all.89 = bf16[4,128,512]{2,1,0:T(8,128)(2,1)S(1)} all-to-all(bf16[4,128,512]{2,1,0:T(8,128)(2,1)S(1)} %bitcast.120), channel_id=1, replica_groups=mesh['ep'=4,'tp'=8] {'ep'}, dimensions={0} | all-to-all | bytes 1048576 | tf_op jit(solution)/shard_map/all_to_all | solution.py:150
  244.0 12.8 %all_to_all.90 = bf16[4,48,2048]{2,1,0:T(8,128)(2,1)} all-to-all(bf16[4,48,2048]{2,1,0:T(8,128)(2,1)} %bitcast.125), channel_id=1, replica_groups=mesh['ep'=4,'tp'=8] {'ep'}, dimensions={0} | all-to-all | bytes 1572864 | tf_op jit(solution)/shard_map/all_to_all | solution.py:133
  256.9 55.6 %reduce-scatter.3.cloned.1.call-done = bf16[192,2048]{1,0:T(8,128)(2,1)} async-done(((bf16[1536,2048]{1,0:T(8,128)(2,1)}), bf16[192,2048]{1,0:T(8,128)(2,1)}) %reduce-scatter.3.cloned.1.call-update) | async-done | bytes 786448 | tf_op jit(solution)/shard_map/reduce_scatter | solution.py:130
  312.5 3.6 %all-to-all-start.4 = ((bf16[4,48,2048]{2,1,0:T(8,128)(2,1)}), bf16[4,48,2048]{2,1,0:T(8,128)(2,1)S(1)}, u32[]{:S(2)}, u32[]{:S(2)}) async-start(bf16[4,48,2048]{2,1,0:T(8,128)(2,1)} %bitcast.126), calls=%async_computation.5 | async-start | bytes 1572864 | tf_op jit(solution)/shard_map/all_to_all | solution.py:133
  317.0 3.0 convolution_bitcast_fusion
  319.9 5.3 %all-to-all-done.4 = bf16[4,48,2048]{2,1,0:T(8,128)(2,1)S(1)} async-done(((bf16[4,48,2048]{2,1,0:T(8,128)(2,1)}), bf16[4,48,2048]{2,1,0:T(8,128)(2,1)S(1)}, u32[]{:S(2)}, u32[]{:S(2)}) %all-to-all-start.4) | async-done | bytes 786464 | tf_op jit(solution)/shard_map/all_to_all | solution.py:133
  325.2 3.1 fusion.39
  (68 shorter events, 9.8 us)
Async XLA Ops:
  7.2 103.1 %copy-start = (bf16[4,2048,128]{2,1,0:T(8,128)(2,1)S(1)}, bf16[4,2048,128]{2,1,0:T(8,128)(2,1)}, u32[]{:S(2)}) copy-start(bf16[4,2048,128]{2,1,0:T(8,128)(2,1)} %param.19) | copy-start | bytes 6291460
  7.2 37.9 %all-gather.4.cloned.1.call-start = ((), (), s32[]{:S(2)}) async-start(), calls=%async_computation.9 | async-start | bytes 1179648 | tf_op jit(solution)/shard_map/all_gather | solution.py:100
  7.2 24.0 %copy-start.1 = (bf16[256,2048]{1,0:T(8,128)(2,1)S(1)}, bf16[256,2048]{1,0:T(8,128)(2,1)}, u32[]{:S(2)}) copy-start(bf16[256,2048]{1,0:T(8,128)(2,1)} %param.13) | copy-start | bytes 3145732
  7.2 24.0 %copy-start.7 = (f32[2048]{0:T(1024)S(1)}, f32[2048]{0:T(1024)}, u32[]{:S(2)}) copy-start(f32[2048]{0:T(1024)} %param.14) | copy-start | bytes 24580
  9.0 92.7 %all-gather.8.cloned.1.call-start = ((), (), s32[]{:S(2)}) async-start(), calls=%async_computation.12 | async-start | bytes 7077888 | tf_op jit(solution)/shard_map/all_gather | solution.py:122
  14.7 30.4 %copy-start.4 = (s32[256,2]{0,1:T(2,128)S(1)}, s32[256,2]{0,1:T(2,128)}, u32[]{:S(2)}) copy-start(s32[256,2]{0,1:T(2,128)} %param.15) | copy-start | bytes 6148
  14.8 30.4 %copy-start.5 = (f32[256,2]{0,1:T(2,128)S(1)}, f32[256,2]{0,1:T(2,128)}, u32[]{:S(2)}) copy-start(f32[256,2]{0,1:T(2,128)} %param.16) | copy-start | bytes 6148
  31.2 135.5 %all-gather.6.cloned.1.call-start = ((), (), s32[]{:S(2)}) async-start(), calls=%async_computation.10 | async-start | bytes 7077888 | tf_op jit(solution)/shard_map/all_gather | solution.py:122
  45.1 199.0 %reduce-scatter.5.cloned.1.call-start = ((), (), s32[]{:S(2)}) async-start(), calls=%async_computation.13 | async-start | bytes 7077888 | tf_op jit(solution)/shard_map/reduce_scatter | solution.py:130
  122.5 189.9 %reduce-scatter.3.cloned.1.call-start = ((), (), s32[]{:S(2)}) async-start(), calls=%async_computation.11 | async-start | bytes 7077888 | tf_op jit(solution)/shard_map/reduce_scatter | solution.py:130
  187.0 0.9 copy-start.3
  188.0 5.1 %copy-start.6 = (f32[128]{0:T(128)S(1)}, f32[128]{0:T(128)}, u32[]{:S(2)}) copy-start(f32[128]{0:T(128)} %param.11) | copy-start | bytes 1540
  188.0 4.8 %collective-permute-start = (bf16[15,128]{1,0:T(8,128)(2,1)S(1)}, bf16[15,128]{1,0:T(8,128)(2,1)S(1)}, u32[]{:S(2)}, u32[]{:S(2)}) collective-permute-start(bf16[15,128]{1,0:T(8,128)(2,1)S(1)} %slice.67), channel_id=1, source_target_pairs={{0,8},{8,16},{16,24},{1,9},{9,17},{17,25},{2,10},{10,18},{18,26},{... | collective-permute-start | bytes 11528 | tf_op jit(solution)/shard_map/ppermute | solution.py:20
  193.1 39.7 %copy-start.2 = (bf16[1024,512]{1,0:T(8,128)(2,1)S(1)}, bf16[1024,512]{1,0:T(8,128)(2,1)}, u32[]{:S(2)}) copy-start(bf16[1024,512]{1,0:T(8,128)(2,1)} %all-gather.4.cloned.1.call-done) | copy-start | bytes 3145732
  312.5 12.7 %all-to-all-start.4 = ((bf16[4,48,2048]{2,1,0:T(8,128)(2,1)}), bf16[4,48,2048]{2,1,0:T(8,128)(2,1)S(1)}, u32[]{:S(2)}, u32[]{:S(2)}) async-start(bf16[4,48,2048]{2,1,0:T(8,128)(2,1)} %bitcast.126), calls=%async_computation.5 | async-start | bytes 1572864 | tf_op jit(solution)/shard_map/all_to_all | solution.py:133
Sparse Core Ops, SparseCore 0:
  10.2 24.9 all-gather.3
  36.8 64.8 all-gather.7
  103.4 63.3 all-gather.5
  168.9 72.5 reduce-scatter.4
  243.7 68.7 reduce-scatter.2
